TPU v7x, 512 devices: a 4x2x32 block of a 4x8x32 slice. The times are simulated.
512 devices in a mesh: grp: 2 (over y), kv: 64 (over z, core), tp: 4 (over x).
Axes of the slice: x: 4, y: 2, z: 32, core: 2. Of those that a mesh axis runs over, the one named last changes fastest.
The devices are a block of a 4x8x32 slice.
Arguments:
- tokens: bfloat16 [65536, 2048], P(('grp', 'kv')), parts along dimension 0, may hold values from -72 to 72
- w_query: bfloat16 [2048, 1024], P(None, 'tp'), may hold values from -0.125 to 0.125
- w_key: bfloat16 [2048, 256], P(None, 'tp'), may hold values from -0.125 to 0.125
- w_value: bfloat16 [2048, 256], P(None, 'tp'), may hold values from -0.125 to 0.125
- w_out: bfloat16 [1024, 2048], P('tp'), may hold values from -0.1875 to 0.1875
- selection: int32 [4, 1024, 32], P('tp', ('grp', 'kv')), parts along dimension 1, may hold values from -1 to 511, as said below
Outputs:
- attended_out: bfloat16 [65536, 2048], P(('grp', 'kv', 'tp')), parts along dimension 0
There are 2 independent parts, one for each index of `grp`. A program takes and returns all parts, laid end to end along the dimension named above; an argument that names none is the same for every part. Nothing has to cross between parts.
Inputs may be any that keep to these rules, and one draw needn't show every extreme that they name: `selection`: entry 0 is the query block's own index; the others are distinct indices of earlier blocks, then -1 for unused entries. For one key head, the query blocks of one device's range together choose at most 2 distinct blocks of any other device's range, and some device reaches 2 in every draw.
All inputs are finite; a program needn't handle non-finite values.
Results may differ from a plain program's by a relative error of at most 0.028.
The roundings to bfloat16 on the way count: a program that leaves them out, or rounds other values in their place, can miss the bound.
Values may be sent and summed in bfloat16 or wider, within the bound.
A program may use at most 128 MiB of HBM per device.

v0:
```python
import jax
import jax.numpy as jnp
from jax import lax
from jax.sharding import PartitionSpec as P

HEAD_DIM = 64
BLOCK = 64
TOPK = 32


ROPE_BASE = 500000.0


def cut_along(shard, dim, peers):
    lengths = shard.shape
    tiles = shard.reshape(*lengths[:dim], peers, lengths[dim] // peers, *lengths[dim + 1 :])
    return jnp.moveaxis(tiles, dim, 0)


def sum_at_owner(shard, axis, dim):
    tiles = cut_along(shard, dim, lax.axis_size(axis))
    arrived = lax.all_to_all(tiles, axis, split_axis=0, concat_axis=0, tiled=True)
    return arrived.astype(jnp.float32).sum(axis=0)


def rotate(head_rows, positions):
    half = head_rows.shape[-1] // 2
    freqs = ROPE_BASE ** (-jnp.arange(half, dtype=jnp.float32) / half)
    angles = positions[:, None, None] * freqs
    cosine = jnp.cos(angles)
    sine = jnp.sin(angles)
    first = head_rows[..., :half]
    second = head_rows[..., half:]
    return jnp.concatenate(
        [first * cosine - second * sine, second * cosine + first * sine], axis=-1
    )


def shards(tokens, w_query, w_key, w_value, w_out, selection):
    row_count = tokens.shape[0]
    local_heads = w_query.shape[1] // HEAD_DIM
    own_index = lax.axis_index("kv")
    positions_int = own_index * row_count + jnp.arange(row_count)
    positions = positions_int.astype(jnp.float32)
    queries = rotate(
        jnp.dot(tokens, w_query, preferred_element_type=jnp.float32).reshape(
            row_count, local_heads, HEAD_DIM
        ),
        positions,
    ).astype(jnp.bfloat16)
    key_local = rotate(
        jnp.dot(tokens, w_key, preferred_element_type=jnp.float32).reshape(row_count, 1, HEAD_DIM),
        positions,
    )[:, 0].astype(jnp.bfloat16)
    value_local = jnp.dot(tokens, w_value, preferred_element_type=jnp.float32).astype(jnp.bfloat16)
    key_value = jnp.concatenate([key_local, value_local], axis=-1)
    blocks_here = row_count // BLOCK
    chosen_ids = selection[0]
    key_table = lax.all_gather(key_value, "kv", axis=0, tiled=True).reshape(-1, BLOCK, 2 * HEAD_DIM)
    slot_ids = jnp.maximum(chosen_ids, 0)
    picked = key_table[slot_ids]
    picked_keys = picked[..., :HEAD_DIM].reshape(blocks_here, TOPK * BLOCK, HEAD_DIM)
    picked_values = picked[..., HEAD_DIM:].reshape(blocks_here, TOPK * BLOCK, HEAD_DIM)
    offsets = jnp.arange(BLOCK)
    key_pos = (chosen_ids[:, :, None] * BLOCK + offsets).reshape(blocks_here, TOPK * BLOCK)
    live_keys = jnp.repeat(chosen_ids >= 0, BLOCK, axis=1)
    query_pos = positions_int.reshape(blocks_here, BLOCK)
    query_rows = queries.reshape(blocks_here, BLOCK, local_heads, HEAD_DIM)
    scores = jnp.einsum(
        "qbhd,qkd->qhbk", query_rows, picked_keys, preferred_element_type=jnp.float32
    ) * HEAD_DIM ** (-0.5)
    allowed = live_keys[:, None, None, :] & (
        key_pos[:, None, None, :] <= query_pos[:, None, :, None]
    )
    scores = jnp.where(allowed, scores, -jnp.inf)
    top_score = jnp.max(scores, axis=-1, keepdims=True)
    expo = jnp.exp(scores - top_score)
    weights = (expo / jnp.sum(expo, axis=-1, keepdims=True)).astype(jnp.bfloat16)
    attended = jnp.einsum(
        "qhbk,qkd->qbhd", weights, picked_values, preferred_element_type=jnp.float32
    ).astype(jnp.bfloat16)
    attended = attended.reshape(row_count, local_heads * HEAD_DIM)
    summed = sum_at_owner(
        jnp.dot(attended, w_out, preferred_element_type=jnp.float32).astype(jnp.bfloat16), "tp", 0
    )
    return summed.astype(jnp.bfloat16)


def solution(mesh):
    placed = (
        P(("grp", "kv"), None),
        P(None, "tp"),
        P(None, "tp"),
        P(None, "tp"),
        P("tp", None),
        P("tp", ("grp", "kv"), None),
    )
    return jax.shard_map(
        shards, mesh=mesh, in_specs=placed, out_specs=P(("grp", "kv", "tp"), None), check_vma=False
    )
```

profile of v0, /device:TPU:33, one launch (start us, length us, event | category | flops | bytes accessed | tf_op | source)
XLA Modules:
  0.0 269.1 jit_solution(14196923973627354760)
XLA Ops:
  6.6 1.6 copy-done
  8.1 1.7 convolution_convert_fusion.1
  9.8 1.7 convolution_bitcast_fusion
  11.6 0.3 fusion.16
  11.9 0.7 pad_maximum_fusion.1
  12.9 0.1 and.16
  13.3 0.3 multiply_cosine_fusion
  13.6 2.0 fusion.27
  15.6 0.2 concatenate.18
  15.8 1.1 copy.12
  17.0 0.2 concatenate.19
  17.2 1.1 copy.13
  18.3 1.0 compare_and_fusion
  19.3 160.9 %all-gather.2.cloned.1.call-done = bf16[32768,128]{0,1:T(8,128)(2,1)} async-done(((bf16[512,128]{0,1:T(8,128)(2,1)}), bf16[32768,128]{0,1:T(8,128)(2,1)}) %all-gather.2.cloned.1.call-update) | async-done | bytes 8388624 | tf_op jit(solution)/shard_map/all_gather | solution.py:59
  180.2 11.9 %copy.9 = bf16[32768,128]{1,0:T(8,128)(2,1)} copy(bf16[32768,128]{0,1:T(8,128)(2,1)} %all-gather.2.cloned.1.call-done) | data formatting | bytes 16777216 | tf_op jit(solution)/shard_map/all_gather | solution.py:59
  192.1 6.4 %gather_fusion = bf16[256,64,128]{2,1,0:T(8,128)(2,1)} fusion(bf16[512,64,128]{2,1,0:T(8,128)(2,1)} %bitcast.53, s32[1024]{0:T(1024)S(1)} %pad_clamp_fusion), kind=kCustom, calls=%fused_computation | custom fusion | bytes 8389632 | tf_op jit(solution)/shard_map/gather | solution.py:61
  198.5 7.3 %fusion.25 = (bf16[8,32,64,64]{3,2,1,0:T(8,128)(2,1)}, bf16[8,32,64,64]{3,2,1,0:T(8,128)(2,1)}) fusion(bf16[8,32,64,128]{3,2,1,0:T(8,128)(2,1)} %bitcast.52), kind=kLoop, calls=%fused_computation.47 | loop fusion | bytes 8388608 | tf_op jit(solution)/shard_map/slice | solution.py:62
  205.8 10.6 %fusion.26 = (f32[8,4,64]{2,1,0:T(4,128)S(1)}, f32[8,4,64,2048]{3,2,1,0:T(8,128)}) fusion(pred[8,64,2048]{2,1,0:T(8,128)(4,1)S(1)} %compare_and_fusion, bf16[8,2048,64,1]{2,1,3,0:T(8,128)(2,1)} %bitcast.56, bf16[8,64,4,32]{3,1,2,0:T(8,128)(2,1)} %copy.13, bf16[8,64,4,32]{3,1,2,0:T(8,128)(2,1)} %copy.12), kind=kOutput, calls=%fused_computation.48 | convolution fusion | flops 554174464 | bytes 20193280 | tf_op jit(solution)/shard_map/sub | solution.py:77
  216.4 10.7 %fusion.9 = bf16[8,64,4,64]{1,3,2,0:T(8,128)(2,1)S(1)} fusion(bf16[8,2048,64,1]{2,1,3,0:T(8,128)(2,1)} %bitcast.55, f32[8,4,64,2048]{3,2,1,0:T(8,128)} %get-tuple-element.16, f32[8,4,64]{2,1,0:T(4,128)S(1)} %get-tuple-element.15), kind=kOutput, calls=%fused_computation.14 | convolution fusion | flops 545390592 | bytes 19144704 | tf_op jit(solution)/shard_map/qhbk,qkd->qbhd/dot_general | solution.py:79
  227.1 0.3 copy.14
  227.5 0.3 reshape.205
  227.8 2.0 convolution_convert_fusion
  229.8 29.6 %all_to_all.5 = bf16[4,128,2048]{2,1,0:T(8,128)(2,1)} all-to-all(bf16[4,128,2048]{2,1,0:T(8,128)(2,1)S(1)} %bitcast.54), channel_id=1, replica_groups=mesh['grp'=2,'kv'=64,'tp'=4] {'tp'}, dimensions={0} | all-to-all | bytes 4194304 | tf_op jit(solution)/shard_map/all_to_all | solution.py:22
  259.4 2.9 %reduce_sum.22 = bf16[128,2048]{1,0:T(8,128)(2,1)} reduce(bf16[4,128,2048]{2,1,0:T(8,128)(2,1)} %all_to_all.5, bf16[]{:T(256)} %constant.29.clone.1), dimensions={0}, to_apply=%region_2.3 | reduce | flops 786432 | bytes 2621442 | tf_op jit(solution)/shard_map/reduce_sum | solution.py:23
  (20 shorter events, 0.6 us)
Async XLA Ops:
  6.5 1.6 copy-start
  6.6 6.1 %copy-start.1 = (s32[1,8,32]{2,1,0:T(8,128)S(1)}, s32[1,8,32]{2,1,0:T(8,128)}, u32[]{:S(2)}) copy-start(s32[1,8,32]{2,1,0:T(8,128)} %param.11) | copy-start | bytes 3076
  6.6 173.6 %all-gather.2.cloned.1.call-start = ((), (), s32[]{:S(2)}) async-start(), calls=%async_computation.1 | async-start | bytes 8519680 | tf_op jit(solution)/shard_map/all_gather | solution.py:59
Sparse Core Ops, SparseCore 0:
  12.8 167.3 all-gather.1
where the time goes:
time: 270 us; the launch traced here: 269 us
  waiting for transfers between devices  161 us (60%)
  local copies, waits for them, and re-layouts  31 us (11%)
  blocking collectives  29.6 us (11%)
  matrix products  28.6 us (11%)
  between operations  13.6 us (5%)
  other arithmetic  5.32 us (2%)
    all_gather x1, waiting for transfers between devices, shards(): lax.all_gather(key_value, 'kv', axis=0, tiled=True)  161 us
    all_to_all x1, blocking collectives, sum_at_owner(): lax.all_to_all(tiles, axis, split_axis=0, concat_axis=0, tiled=True)  29.6 us
    all_gather x1, local copies, waits for them, and re-layouts, shards(): lax.all_gather(key_value, 'kv', axis=0, tiled=True)  11.9 us
    dot_general x1, matrix products, shards(): jnp.einsum('qhbk,qkd->qbhd', weights, picked_values, preferred_element_ty...  10.7 us
    sub x1, matrix products, shards(): expo = jnp.exp(scores - top_score)  10.6 us
    slice x1, local copies, waits for them, and re-layouts, shards(): picked[..., :HEAD_DIM].reshape(blocks_here, TOPK * BLOCK, HEAD_DIM)  7.28 us
    gather x1, local copies, waits for them, and re-layouts, shards(): picked = key_table[slot_ids]  6.41 us
  transfers between devices with their start and end apart: 1, of which 1 were waited for; matrix products, arithmetic and copies ran while one was open for 2% of the time, Pallas kernels for 0%

commit v1 on v0

v1 whole, which is shorter than its diff:
```python
import functools
import math

import jax
import jax.numpy as jnp
import numpy as np
from jax import lax
from jax.experimental import pallas as pl
from jax.experimental.pallas import tpu as pltpu
from jax.sharding import PartitionSpec as P

HEAD_DIM = 64
BLOCK = 64
ROPE_BASE = 500000.0
CORES = 2
LANES = 128
CHUNKS = 8
TILES = 8
TCOLS = 256
SCALE = math.log2(math.e) * HEAD_DIM**-0.5
NEG = float("-inf")


def kernel(
    nkv, ntp,
    tok, wq, wk, wv, wo, cr, sr, sel, cb, sb,
    out,
    tok_v, wq_v, wkv_v, wall, cr_v, sr_v, kv, qt, acc, mx, kvs, wt, sbuf, biasr, ownb, tab_v, tab_s,
    att, att_in, oacc, ov,
    in_sem, tok_sem, ring_send, ring_recv, sib_send, sib_recv, w_send, w_recv, w_sib, a_send, a_recv, o_sem, t_sem,
):
    rows = tok.shape[0]
    crows = rows // CHUNKS
    pairs = rows // LANES
    nchip = nkv // CORES
    far = nchip // 2
    me = lax.axis_index("kv")
    core = lax.rem(me, CORES)
    z = me // CORES
    g = lax.axis_index("tp")
    sibling = z * CORES + (1 - core)
    right, left, opposite = lax.rem(g + 1, ntp), lax.rem(g + ntp - 1, ntp), lax.rem(g + 2, ntp)

    def dev(dist, c):
        return lax.rem(z + dist + 2 * nchip, nchip) * CORES + c

    loads = [
        pltpu.make_async_copy(wk, wkv_v.at[pl.ds(0, HEAD_DIM)], in_sem.at[0]),
        pltpu.make_async_copy(wv, wkv_v.at[pl.ds(HEAD_DIM, HEAD_DIM)], in_sem.at[1]),
    ]
    tok_loads = [
        pltpu.make_async_copy(tok.at[pl.ds(i * LANES, LANES)], tok_v.at[pl.ds(i * LANES, LANES)], tok_sem.at[i])
        for i in range(pairs)
    ]
    cr_load = pltpu.make_async_copy(cr, cr_v, in_sem.at[2])
    sr_load = pltpu.make_async_copy(sr, sr_v, in_sem.at[3])
    wq_load = pltpu.make_async_copy(wq, wq_v, in_sem.at[4])
    wo_load = pltpu.make_async_copy(wo, wall.at[g], in_sem.at[5])
    loads[0].start()
    loads[1].start()
    tok_loads[0].start()
    cr_load.start()
    sr_load.start()
    for i in range(1, pairs):
        tok_loads[i].start()
    wq_load.start()
    wo_load.start()

    barrier = pltpu.get_barrier_semaphore()
    for target in ({"kv": dev(1, core)}, {"kv": dev(-1, core)}, {"kv": sibling}, {"tp": right}, {"tp": left}, {"tp": opposite}):
        pl.semaphore_signal(barrier, inc=1, device_id=target)

    def ring(way, t, ch, source):
        span = pl.ds(pl.multiple_of(source * rows + ch * crows, crows), crows)
        return pltpu.make_async_remote_copy(
            src_ref=kv.at[span], dst_ref=kv.at[span], send_sem=ring_send.at[way], recv_sem=ring_recv.at[way, t, ch],
            device_id={"kv": dev(1 if way == 0 else -1, core)},
        )

    def ring_source(way, t):
        return dev(-t if way == 0 else t, core)

    def to_sibling(t, ch, source):
        span = pl.ds(pl.multiple_of(source * rows + ch * crows, crows), crows)
        return pltpu.make_async_remote_copy(
            src_ref=kv.at[span], dst_ref=kv.at[span], send_sem=sib_send.at[0], recv_sem=sib_recv.at[t],
            device_id={"kv": sibling},
        )

    def wait_sibling(t, count):
        span = pl.ds(0, count)
        pltpu.make_async_remote_copy(
            src_ref=kv.at[span], dst_ref=kv.at[span], send_sem=sib_send.at[0], recv_sem=sib_recv.at[t],
            device_id={"kv": sibling},
        ).wait_recv()

    wrows = wall.shape[1]
    half = wrows // CORES
    quarter = half // 2

    def w_copy(group, first, count, sem, recv, target):
        span = pl.ds(pl.multiple_of(first, quarter), count)
        return pltpu.make_async_remote_copy(
            src_ref=wall.at[group, span], dst_ref=wall.at[group, span], send_sem=w_send.at[sem], recv_sem=recv,
            device_id=target,
        )

    h0 = core * half
    w1 = [
        w_copy(g, h0, half, 0, w_recv.at[0], {"tp": right}),
        w_copy(g, h0, half, 1, w_recv.at[1], {"tp": left}),
    ]
    w2 = [
        w_copy(left, h0, quarter, 2, w_recv.at[2], {"tp": right}),
        w_copy(right, h0 + quarter, quarter, 3, w_recv.at[3], {"tp": left}),
        w_copy(left, h0, half, 4, w_sib.at[0], {"kv": sibling}),
        w_copy(right, h0, half, 5, w_sib.at[1], {"kv": sibling}),
    ]
    w3 = [w_copy(opposite, h0, half, 6, w_sib.at[2], {"kv": sibling})]

    lane = lax.broadcasted_iota(jnp.int32, (1, LANES), 1)
    sign = jnp.where(lax.rem(lane, HEAD_DIM) < HEAD_DIM // 2, -1.0, 1.0)
    first_half = lax.rem(lane, HEAD_DIM) < HEAD_DIM // 2
    is_key = lane < HEAD_DIM
    cb_row = cb[pl.ds(me, 1), :]
    sb_row = sb[pl.ds(me, 1), :]

    def angles(i):
        span = pl.ds(i * LANES, LANES)
        cr_t, sr_t = cr_v[span, :], sr_v[span, :]
        cosine = cb_row * cr_t - sb_row * sr_t
        sine = (sb_row * cr_t + cb_row * sr_t) * sign
        return cosine, sine

    def swapped(x):
        return jnp.where(first_half, pltpu.roll(x, LANES - HEAD_DIM // 2, 1), pltpu.roll(x, HEAD_DIM // 2, 1))

    loads[0].wait()
    loads[1].wait()
    for i in range(pairs):
        tok_loads[i].wait()
        x = lax.dot_general(
            tok_v[pl.ds(i * LANES, LANES), :], wkv_v[...], (((1,), (1,)), ((), ())), preferred_element_type=jnp.float32
        )
        if i == 0:
            cr_load.wait()
            sr_load.wait()
        cosine, sine = angles(i)
        rotated = x * jnp.where(is_key, cosine, 1.0) + swapped(x) * jnp.where(is_key, sine, 0.0)
        kv[pl.ds(pl.multiple_of(me * rows + i * LANES, LANES), LANES), :] = rotated.astype(jnp.bfloat16)
        if i == 0:
            pl.semaphore_wait(barrier, 6)
        for ch in range(i * LANES // crows, (i + 1) * LANES // crows):
            ring(0, 1, ch, me).start()
            ring(1, 1, ch, me).start()
            to_sibling(0, ch, me).start()
    wo_load.wait()
    for copy in w1:
        copy.start()

    nblocks = rows // BLOCK
    chosen = sel[0]
    lanes8 = lax.broadcasted_iota(jnp.int32, (nblocks, LANES), 1)
    bits = jnp.zeros((nblocks, LANES), jnp.int32)
    for t in range(chosen.shape[1]):
        entry = jnp.broadcast_to(chosen[:, t : t + 1], (nblocks, LANES))
        for j in range(nblocks):
            bits = bits | jnp.where(entry == lanes8 * nblocks + j, 1 << j, 0)
    union = bits[0:1]
    for b in range(1, nblocks):
        union = union | bits[b : b + 1]
    union = jnp.broadcast_to(union, (nblocks, LANES))
    low = union & (-union)
    rest = union & ~low
    low2 = rest & (-rest)
    index = jnp.zeros_like(union)
    for j in range(1, nblocks):
        index = index + jnp.where(low == (1 << j), j, 0) + jnp.where(low2 == (1 << j), j * 256, 0)
    tab_v[0:8, :] = bits
    tab_v[8:16, :] = index
    tab_copy = pltpu.make_async_copy(tab_v, tab_s, t_sem.at[0])
    tab_copy.start()
    for slot, bit in enumerate((low, low2)):
        open_ = jnp.where((bits & bit) != 0, 0.0, NEG)
        turned = open_.T[:nkv]
        for p in range(pairs):
            biasr[slot * pairs + p] = jnp.where(
                is_key,
                jnp.broadcast_to(turned[:, 2 * p : 2 * p + 1], (nkv, LANES)),
                jnp.broadcast_to(turned[:, 2 * p + 1 : 2 * p + 2], (nkv, LANES)),
            )

    wq_load.wait()
    heads = wq_v.shape[1] // HEAD_DIM
    for i in range(pairs):
        x = jnp.dot(tok_v[pl.ds(i * LANES, LANES), :], wq_v[...], preferred_element_type=jnp.float32)
        cosine, sine = angles(i)
        for hp in range(heads // 2):
            part = x[:, hp * LANES : (hp + 1) * LANES]
            rotated = (part * cosine + swapped(part) * sine).astype(jnp.bfloat16).astype(jnp.float32)
            flipped = rotated.T.astype(jnp.bfloat16)
            u = i * 2 + hp
            qt[u, 0:HEAD_DIM, 0:LANES] = flipped[:HEAD_DIM]
            qt[u, 0:HEAD_DIM, LANES:TCOLS] = flipped[HEAD_DIM:]
            qt[u, HEAD_DIM:LANES, :] = jnp.zeros((LANES - HEAD_DIM, TCOLS), jnp.bfloat16)

    tab_copy.wait()
    key_row = lax.broadcasted_iota(jnp.int32, (BLOCK, LANES), 0)
    query_col = lax.rem(lax.broadcasted_iota(jnp.int32, (BLOCK, LANES), 1), BLOCK)
    causal = jnp.where(key_row <= query_col, 0.0, NEG)
    for p in range(pairs):
        for j in range(2 * p + 2):
            sides = []
            for b in (2 * p, 2 * p + 1):
                if j > b:
                    sides.append(jnp.full((BLOCK, LANES), NEG, jnp.float32))
                else:
                    seen = (tab_s[b, me] >> j) & 1
                    gate = jnp.where(seen == 1, 0.0, NEG)
                    sides.append((causal if j == b else jnp.zeros((BLOCK, LANES), jnp.float32)) + gate)
            ownb[p, j * BLOCK : (j + 1) * BLOCK, :] = jnp.where(is_key, sides[0], sides[1])

    def chosen_blocks(source):
        packed = tab_s[8, source]
        i0, i1 = packed & 255, packed >> 8
        base = source * rows
        first = second = kv[pl.ds(pl.multiple_of(base, BLOCK), BLOCK), :]
        for j in range(1, nblocks):
            block = kv[pl.ds(pl.multiple_of(base + j * BLOCK, BLOCK), BLOCK), :]
            first = lax.select_n(i0 == j, first, block)
            second = lax.select_n(i1 == j, second, block)
        return first, second

    def gather(sources, at=0):
        for n, source in enumerate(sources):
            first, second = chosen_blocks(source)
            o = at + n * 2 * BLOCK
            kvs[o : o + BLOCK, :] = first
            kvs[o + BLOCK : o + 2 * BLOCK, :] = second

    def turn(count):
        values = jnp.where(lane < HEAD_DIM, jnp.ones((), jnp.bfloat16), kvs[0:count, :])
        wt[:, 0:count] = values.T

    def scores(u, count):
        sbuf[u % 2, 0:count, :] = jnp.dot(kvs[0:count, :], qt[u], preferred_element_type=jnp.float32)

    def twice(row):
        return jnp.concatenate([row, row], axis=1)

    def remote_bias(u, sources):
        found = []
        for source in sources:
            for slot in (0, 1):
                found.append(twice(biasr[slot * pairs + u // 2, pl.ds(source, 1), :]))
        return found

    def attend(u, count, biases, first=False):
        blocks, tops = [], []
        for k in range(count // BLOCK):
            sk = sbuf[u % 2, k * BLOCK : (k + 1) * BLOCK, :]
            bias = biases[k]
            if bias.shape[0] > 1:
                sk = sk + bias
                bias = None
            top = jnp.max(sk, axis=0, keepdims=True)
            tops.append(top if bias is None else top + bias)
            blocks.append((sk, bias))
        m_new = functools.reduce(jnp.maximum, tops)
        if not first:
            m_old = mx[u]
            m_new = jnp.maximum(m_new, m_old)
            alpha = jnp.exp2((m_old - m_new) * SCALE)
        probs = []
        for sk, bias in blocks:
            shift = m_new if bias is None else m_new - bias
            probs.append(jnp.exp2((sk - shift) * SCALE).astype(jnp.bfloat16))
        gained = jnp.dot(wt[:, 0:count], jnp.concatenate(probs, axis=0), preferred_element_type=jnp.float32)
        acc[u] = gained if first else acc[u] * alpha + gained
        mx[u] = m_new

    def receive(t, u, forward_up=True, forward_down=True):
        for way, forward in ((0, forward_up), (1, forward_down)):
            source = ring_source(way, t)
            ring(way, t, u, source).wait_recv()
            if forward is True:
                ring(way, t + 1, u, source).start()
            elif forward is not False:
                @pl.when(forward)
                def _():
                    ring(way, t + 1, u, source).start()
            to_sibling(t, u, source).start()

    for u in range(TILES):
        receive(1, u)
        p = u // 2
        own_keys = (2 * p + 2) * BLOCK
        count = own_keys + 2 * BLOCK
        if u == 0:
            wait_sibling(0, rows)
        if u % 2 == 0:
            kvs[0:own_keys, :] = kv[pl.ds(pl.multiple_of(me * rows, rows), own_keys), :]
            gather([sibling], own_keys)
            turn(count)
        scores(u, count)
        own = [
            jnp.concatenate([ownb[p, j * BLOCK : (j + 1) * BLOCK, :]] * 2, axis=1) for j in range(2 * p + 2)
        ]
        attend(u, count, own + remote_bias(u, [sibling]), first=True)

    def four(t):
        return [dev(-t, 0), dev(-t, 1), dev(t, 0), dev(t, 1)]

    def round_(t, receive_tile):
        sources = four(t - 1)
        count = len(sources) * 2 * BLOCK
        for u in range(TILES):
            receive_tile(u)
            if u == 0:
                wait_sibling(t - 1, 2 * rows)
                gather(sources)
                turn(count)
                scores(0, count)
            if u + 1 < TILES:
                scores(u + 1, count)
            attend(u, count, remote_bias(u, sources))

    def middle(t, carry):
        @pl.when(t == 6)
        def _():
            for copy in w1:
                copy.wait_recv()
            for copy in w2:
                copy.start()

        @pl.when(t == 11)
        def _():
            for copy in w2[:2]:
                copy.wait_recv()
            for copy in w3:
                copy.start()

        def receive_tile(u):
            more = t + 1 < far
            receive(t, u, True if u < CHUNKS // 2 else more, more if u < CHUNKS // 2 else True)

        round_(t, receive_tile)
        return carry

    lax.fori_loop(2, far, middle, 0)

    def last_receive(u):
        if u < CHUNKS // 2:
            for way, ch in ((0, u), (1, u + CHUNKS // 2)):
                source = ring_source(way, far)
                ring(way, far, ch, source).wait_recv()
                to_sibling(far, ch, source).start()

    round_(far, last_receive)

    sources = [dev(far, 0), dev(far, 1)]
    count = len(sources) * 2 * BLOCK
    wait_sibling(far, rows)
    gather(sources)
    turn(count)
    scores(0, count)

    def a_copy(pair, d):
        return pltpu.make_async_remote_copy(
            src_ref=att.at[pair], dst_ref=att_in.at[g], send_sem=a_send.at[d], recv_sem=a_recv.at[d],
            device_id={"tp": pair},
        )

    for u in range(TILES):
        if u + 1 < TILES:
            scores(u + 1, count)
        attend(u, count, remote_bias(u, sources))
        done = acc[u]
        share = (done[HEAD_DIM:] / done[:HEAD_DIM]).astype(jnp.bfloat16)
        pair, hp = u // 2, u % 2
        for hh in range(2):
            first = (hp * 2 + hh) * HEAD_DIM
            att[pair, first : first + HEAD_DIM, :] = share[:, hh * LANES : (hh + 1) * LANES]
        if hp == 1:
            @pl.when(pair != g)
            def _():
                a_copy(pair, lax.rem(pair - g + ntp, ntp)).start()

    for n in range(3):
        w_copy((left, right, opposite)[n], h0, half, 4 + n, w_sib.at[n], {"kv": sibling}).wait_recv()
    ocols = 512
    steps = ov.shape[1] // ocols
    for n, d in enumerate((0, 1, 3, 2)):
        source = lax.rem(g - d + ntp, ntp)
        if d == 0:
            part = att[g]
        else:
            pltpu.make_async_remote_copy(
                src_ref=att.at[g], dst_ref=att_in.at[source], send_sem=a_send.at[d], recv_sem=a_recv.at[d],
                device_id={"tp": source},
            ).wait_recv()
            part = att_in[source]
        part = part.T
        for s in range(steps):
            cols = pl.ds(s * ocols, ocols)
            product = jnp.dot(part, wall[source, :, cols], preferred_element_type=jnp.float32)
            product = product.astype(jnp.bfloat16).astype(jnp.float32)
            if n == 0:
                oacc[:, cols] = product
            elif n < 3:
                oacc[:, cols] = oacc[:, cols] + product
            else:
                ov[:, cols] = (oacc[:, cols] + product).astype(jnp.bfloat16)
                pltpu.make_async_copy(ov.at[:, cols], out.at[:, cols], o_sem.at[s]).start()

    for d in (1, 2, 3):
        a_copy(lax.rem(g + d, ntp), d).wait_send()
    for copy in w1 + w2 + w3:
        copy.wait_send()
    sent = rows * (far - 1) + rows // 2
    for way in (0, 1):
        span = pl.ds(0, sent)
        pltpu.make_async_remote_copy(
            src_ref=kv.at[span], dst_ref=kv.at[span], send_sem=ring_send.at[way], recv_sem=ring_recv.at[way, 0, 0],
            device_id={"kv": sibling},
        ).wait_send()
    span = pl.ds(0, rows * nchip)
    pltpu.make_async_remote_copy(
        src_ref=kv.at[span], dst_ref=kv.at[span], send_sem=sib_send.at[0], recv_sem=sib_recv.at[0],
        device_id={"kv": sibling},
    ).wait_send()
    for s in range(steps):
        cols = pl.ds(s * ocols, ocols)
        pltpu.make_async_copy(ov.at[:, cols], out.at[:, cols], o_sem.at[s]).wait()


def rotary_tables(rows, nkv):
    half = HEAD_DIM // 2
    freqs = ROPE_BASE ** (-np.arange(half, dtype=np.float64) / half)
    freqs = np.tile(freqs, LANES // half)[None, :]
    within = np.arange(rows, dtype=np.float64)[:, None] * freqs
    base = (np.arange(nkv, dtype=np.float64) * rows)[:, None] * freqs
    return [f(a).astype(np.float32) for a in (within, base) for f in (np.cos, np.sin)]


def solution(mesh):
    nkv, ntp = mesh.shape["kv"], mesh.shape["tp"]
    far = nkv // CORES // 2

    def shards(tokens, w_query, w_key, w_value, w_out, selection):
        rows, width = tokens.shape
        pairs = rows // LANES
        crow, srow, cbase, sbase = rotary_tables(rows, nkv)
        anywhere = pl.BlockSpec(memory_space=pl.ANY)
        vmem = pl.BlockSpec(memory_space=pltpu.VMEM)
        wide = w_out.shape[1]
        bf16, f32, i32 = jnp.bfloat16, jnp.float32, jnp.int32
        dma = pltpu.SemaphoreType.DMA
        return pl.pallas_call(
            functools.partial(kernel, nkv, ntp),
            out_shape=jax.ShapeDtypeStruct((rows // ntp, wide), bf16),
            in_specs=[anywhere] * 7 + [vmem] * 3,
            out_specs=anywhere,
            scratch_shapes=[
                pltpu.VMEM(tokens.shape, bf16),
                pltpu.VMEM(w_query.shape, bf16),
                pltpu.VMEM((2 * HEAD_DIM, width), bf16),
                pltpu.VMEM((ntp, *w_out.shape), bf16),
                pltpu.VMEM((rows, LANES), f32),
                pltpu.VMEM((rows, LANES), f32),
                pltpu.VMEM((nkv * rows, 2 * HEAD_DIM), bf16),
                pltpu.VMEM((TILES, LANES, TCOLS), bf16),
                pltpu.VMEM((TILES, LANES, TCOLS), f32),
                pltpu.VMEM((TILES, 1, TCOLS), f32),
                pltpu.VMEM((rows + 2 * BLOCK, LANES), bf16),
                pltpu.VMEM((LANES, rows + 2 * BLOCK), bf16),
                pltpu.VMEM((2, rows + 2 * BLOCK, TCOLS), f32),
                pltpu.VMEM((2 * pairs, nkv, LANES), f32),
                pltpu.VMEM((pairs, rows, LANES), f32),
                pltpu.VMEM((16, LANES), i32),
                pltpu.SMEM((16, LANES), i32),
                pltpu.VMEM((pairs, w_query.shape[1], LANES), bf16),
                pltpu.VMEM((pairs, w_query.shape[1], LANES), bf16),
                pltpu.VMEM((rows // ntp, wide), f32),
                pltpu.VMEM((rows // ntp, wide), bf16),
                dma((6,)),
                dma((pairs,)),
                dma((2,)),
                dma((2, far + 1, CHUNKS)),
                dma((1,)),
                dma((far + 1,)),
                dma((7,)),
                dma((4,)),
                dma((3,)),
                dma((ntp,)),
                dma((ntp,)),
                dma((wide // 512,)),
                dma((1,)),
            ],
            compiler_params=pltpu.CompilerParams(
                collective_id=0, has_side_effects=True, vmem_limit_bytes=60 * 1024 * 1024
            ),
        )(tokens, w_query, w_key.T, w_value.T, w_out, crow, srow, selection, cbase, sbase)

    placed = (
        P(("grp", "kv"), None),
        P(None, "tp"),
        P(None, "tp"),
        P(None, "tp"),
        P("tp", None),
        P("tp", ("grp", "kv"), None),
    )
    return jax.shard_map(
        shards, mesh=mesh, in_specs=placed, out_specs=P(("grp", "kv", "tp"), None), check_vma=False
    )
```

time: 270 us -> 123 us (0.46)
  waiting for transfers between devices: 161 us -> 0 us
  Pallas kernels: 0 us -> 121 us
  blocking collectives: 29.6 us -> 0 us
  local copies, waits for them, and re-layouts: 31 us -> 1.88 us
  matrix products: 28.6 us -> 0 us
  between operations: 13.6 us -> 0.01 us
  other arithmetic: 5.32 us -> 0 us
    all_gather x1 -> x0, waiting for transfers between devices: 161 us -> none  [shards(): lax.all_gather(key_value, 'kv', axis=0, tiled=True)]
    pallas_call x0 -> x1, Pallas kernels: none -> 121 us  [shards(): pl.pallas_call(functools.partial(kernel, nkv, ntp), out_shape=jax.ShapeDt...]
    all_to_all x1 -> x0, blocking collectives: 29.6 us -> none  [sum_at_owner(): lax.all_to_all(tiles, axis, split_axis=0, concat_axis=0, tiled=True)]
    dot_general x5 -> x0, matrix products: 18 us -> none  [the longest x1 10.7 us: shards(): jnp.einsum('qhbk,qkd->qbhd', weights, picked_values, preferred_element_ty...]
    all_gather x1 -> x0, local copies, waits for them, and re-layouts: 11.9 us -> none  [shards(): lax.all_gather(key_value, 'kv', axis=0, tiled=True)]
    sub x1 -> x0, matrix products: 10.6 us -> none  [shards(): expo = jnp.exp(scores - top_score)]
    slice x1 -> x0, local copies, waits for them, and re-layouts: 7.28 us -> none  [shards(): picked[..., :HEAD_DIM].reshape(blocks_here, TOPK * BLOCK, HEAD_DIM)]
    gather x1 -> x0, local copies, waits for them, and re-layouts: 6.41 us -> none  [shards(): picked = key_table[slot_ids]]
  transfers between devices with their start and end apart: 1 -> 0, of which waited for: 1 -> 0; matrix products, arithmetic and copies ran while one was open for 2% -> 0% of each run, Pallas kernels for 0% -> 0%
where the time goes in v1:
time: 123 us
  Pallas kernels  121 us (98%)
  local copies, waits for them, and re-layouts  1.88 us (2%)
    pallas_call x1, Pallas kernels, shards(): pl.pallas_call(functools.partial(kernel, nkv, ntp), out_shape=jax.ShapeDt...  121 us

profile of v1, /device:TPU:33, one launch (start us, length us, event | category | flops | bytes accessed | tf_op | source)
XLA Modules:
  0.0 122.7 jit_solution(2521746045234153973)
XLA Ops:
  0.0 120.8 %shard_map.100 = bf16[128,2048]{1,0:T(8,128)(2,1)} custom-call(bf16[512,2048]{1,0:T(8,128)(2,1)} %tok.1, bf16[2048,256]{1,0:T(8,128)(2,1)} %wq.1, bf16[64,2048]{1,0:T(8,128)(2,1)} %bitcast.2, bf16[64,2048]{1,0:T(8,128)(2,1)} %bitcast.3, bf16[256,2048]{1,0:T(8,128)(2,1)} %wo.1, f32[512,128]{1,0:T(8,128)} %constant.8.clone.cr, f32[512,128]{1,0:T(8,128)} %constant.9.clone.sr, ...), custom_call_target="tpu_custom_call" | custom-call | tf_op jit(solution)/shard_map/pallas_call | solution.py:459
  120.8 1.9 %copy.12 = bf16[128,2048]{1,0:T(8,128)(2,1)} copy(bf16[128,2048]{1,0:T(8,128)(2,1)} %shard_map.100) | data formatting | bytes 1048576
